TPU v7x, 32 devices: a whole 2x2x4 slice. The times are simulated.
32 devices in a mesh: gr: 2 (over x), sp: 8 (over z, y), tp: 2 (over core).
Axes of the slice: x: 2, y: 2, z: 4, core: 2. Of those that a mesh axis runs over, the one named last changes fastest.
Arguments:
- prompt_block_input: bfloat16 [16, 2048, 2048], P('gr', 'sp'), may hold values from -6 to 6
- key_projection_weight: bfloat16 [2048, 512], P(None, 'tp'), may hold values from -0.125 to 0.125
- value_projection_weight: bfloat16 [2048, 512], P(None, 'tp'), may hold values from -0.125 to 0.125
- forget_gate_weight: bfloat16 [8, 2048], P('tp'), may hold values from -0.125 to 0.125
- forget_gate_bias: float32 [8], P('tp'), may hold values from 3.5 to 12
- forget_gate_scale: float32 [16, 8, 2048], P('gr', 'tp', 'sp'), may hold values from 0.15 to 6
- gate_spike_added: float32 [16, 8, 2048], P('gr', 'tp', 'sp'), may hold values from -0.7 to 0
- prior_key_value_cache: bfloat16 [16, 14336, 8, 128], P(('gr', 'sp'), None, 'tp')
- prior_cumulative_log_forget: float32 [16, 8, 14336], P(('gr', 'sp'), 'tp'), as said below
- decoded_token_query: bfloat16 [16, 1024], P('gr', 'tp')
- decoded_token_key: bfloat16 [16, 512], P(('gr', 'sp'), 'tp'), may hold values from -6 to 6
- decoded_token_value: bfloat16 [16, 512], P(('gr', 'sp'), 'tp'), may hold values from -6 to 6
- decoded_log_gate: float32 [16, 8], P(('gr', 'sp'), 'tp'), may hold values from -2.5 to -0.05
- key_norm_gain: float32 [64], replicated, may hold values from 0.1 to 1.9
- read_norm_gain: float32 [1024], P('tp'), may hold values from 0.1 to 1.9
Outputs:
- new_cache: bfloat16 [16, 2048, 8, 128], P(('gr', 'sp'), None, 'tp')
- new_logc: float32 [16, 8, 2048], P(('gr', 'sp'), 'tp')
- next_read: bfloat16 [16, 1024], P(('gr', 'sp'), 'tp')
Inputs may be any that keep to these rules, and one draw needn't show every extreme that they name: `prior_cumulative_log_forget`: each position's cumulative log forget value from the start of its sequence.
All inputs are finite; a program needn't handle non-finite values.
Results may differ from a plain program's by a relative error of at most 0.008.
Values may be sent and summed in bfloat16 or wider, within the bound.
A program may use at most 128 MiB of HBM per device.

v0:
```python
import jax
import jax.numpy as jnp
from jax import lax
from jax.sharding import PartitionSpec as P

EPSILON = 1e-06


def project(
    tok_rows,
    key_projection_weight,
    value_projection_weight,
    forget_gate_weight,
    forget_gate_bias,
    key_norm_gain,
):
    head_dim = key_norm_gain.shape[0]
    key_raw = jnp.einsum(
        "spd,dc->spc", tok_rows, key_projection_weight, preferred_element_type=jnp.float32
    )
    split_heads = key_raw.reshape(key_raw.shape[:2] + (-1, head_dim))
    normed = (
        split_heads
        * lax.rsqrt(jnp.mean(split_heads * split_heads, axis=-1, keepdims=True) + EPSILON)
        * key_norm_gain
    )
    block_keys = normed.astype(jnp.bfloat16)
    block_values = jnp.einsum(
        "spd,dc->spc", tok_rows, value_projection_weight, preferred_element_type=jnp.float32
    )
    block_values = block_values.reshape(split_heads.shape).astype(jnp.bfloat16)
    cache_rows = jnp.concatenate([block_keys, block_values], axis=-1)
    gate_preactivation = jnp.einsum(
        "spd,hd->shp", tok_rows, forget_gate_weight, preferred_element_type=jnp.float32
    )
    return (cache_rows, gate_preactivation + forget_gate_bias[None, :, None])


def forget_value_rows(gate_preactivation, forget_gate_scale, gate_spike_added):
    return forget_gate_scale * jax.nn.log_sigmoid(gate_preactivation) + gate_spike_added


def query_split(query, kv_count, head_dim):
    return query.reshape(query.shape[0], kv_count, -1, head_dim)


def head_scores(query, cache_rows, head_dim):
    query_heads = query_split(query, cache_rows.shape[2], head_dim)
    key_heads = cache_rows[..., :head_dim]
    return jnp.einsum(
        "skge,slke->skgl", query_heads, key_heads, preferred_element_type=jnp.float32
    ) * head_dim ** (-0.5)


def weigh(scores, cache_rows, head_dim):
    row_top = jnp.max(scores, axis=-1)
    weights = jnp.exp(scores - row_top[..., None]).astype(jnp.bfloat16)
    value_heads = cache_rows[..., head_dim:]
    return (
        row_top,
        jnp.einsum("skgl,slke->skge", weights, value_heads, preferred_element_type=jnp.float32),
    )


def local(
    prompt_block_input,
    key_projection_weight,
    value_projection_weight,
    forget_gate_weight,
    forget_gate_bias,
    forget_gate_scale,
    gate_spike_added,
    prior_key_value_cache,
    prior_cumulative_log_forget,
    decoded_token_query,
    decoded_token_key,
    decoded_token_value,
    decoded_log_gate,
    key_norm_gain,
    read_norm_gain,
):
    head_dim = key_norm_gain.shape[0]
    own_count = prior_key_value_cache.shape[0]
    kv_count = prior_key_value_cache.shape[2]
    seq_start = lax.axis_index("sp") * own_count
    query_own = lax.dynamic_slice_in_dim(decoded_token_query, seq_start, own_count, 0)
    rows_local, gate_preactivation = project(
        prompt_block_input,
        key_projection_weight,
        value_projection_weight,
        forget_gate_weight,
        forget_gate_bias,
        key_norm_gain,
    )
    local_forget_values = forget_value_rows(gate_preactivation, forget_gate_scale, gate_spike_added)
    new_cache = lax.all_to_all(rows_local, "sp", split_axis=0, concat_axis=1, tiled=True)
    log_forget_value = lax.all_to_all(
        local_forget_values, "sp", split_axis=0, concat_axis=2, tiled=True
    )
    new_logc = prior_cumulative_log_forget[:, :, -1:] + jnp.cumsum(log_forget_value, axis=-1)
    final_logc = new_logc[:, :, -1] + decoded_log_gate
    past_scores = (
        head_scores(query_own, prior_key_value_cache, head_dim)
        + final_logc[:, :, None, None]
        - prior_cumulative_log_forget[:, :, None, :]
    )
    past_top, past_sum = weigh(past_scores, prior_key_value_cache, head_dim)
    block_scores = (
        head_scores(query_own, new_cache, head_dim)
        + final_logc[:, :, None, None]
        - new_logc[:, :, None, :]
    )
    block_top, block_sum = weigh(block_scores, new_cache, head_dim)
    query_heads = query_split(query_own, kv_count, head_dim)
    own_keys = decoded_token_key.reshape(own_count, kv_count, head_dim)
    own_score = jnp.einsum(
        "skge,ske->skg", query_heads, own_keys, preferred_element_type=jnp.float32
    ) * head_dim ** (-0.5)
    row_top = jnp.maximum(jnp.maximum(past_top, block_top), own_score)
    own_weight = jnp.exp(own_score - row_top).astype(jnp.bfloat16)
    weighted = (
        past_sum * jnp.exp(past_top - row_top)[..., None]
        + block_sum * jnp.exp(block_top - row_top)[..., None]
    )
    own_values = decoded_token_value.reshape(own_count, kv_count, 1, head_dim).astype(jnp.float32)
    weighted = weighted + own_weight.astype(jnp.float32)[..., None] * own_values
    normed = weighted * lax.rsqrt(jnp.mean(weighted * weighted, axis=-1, keepdims=True) + EPSILON)
    next_read = (normed.reshape(own_count, -1) * read_norm_gain).astype(jnp.bfloat16)
    return (new_cache, new_logc, next_read)


def solution(mesh):
    return jax.shard_map(
        local,
        mesh=mesh,
        in_specs=(
            P("gr", "sp", None),
            P(None, "tp"),
            P(None, "tp"),
            P("tp", None),
            P("tp"),
            P("gr", "tp", "sp"),
            P("gr", "tp", "sp"),
            P(("gr", "sp"), None, "tp", None),
            P(("gr", "sp"), "tp", None),
            P("gr", "tp"),
            P(("gr", "sp"), "tp"),
            P(("gr", "sp"), "tp"),
            P(("gr", "sp"), "tp"),
            P(),
            P("tp"),
        ),
        out_specs=(
            P(("gr", "sp"), None, "tp", None),
            P(("gr", "sp"), "tp", None),
            P(("gr", "sp"), "tp"),
        ),
        check_vma=False,
    )
```

profile of v0, /device:TPU:0, one launch (start us, length us, event | category | flops | bytes accessed | tf_op | source)
XLA Modules:
  0.0 118.0 jit_solution(34637716511074179)
XLA Ops:
  0.6 0.0 copy-start
  0.6 6.4 %fusion.20 = f32[8,4,256]{2,1,0:T(4,128)} fusion(f32[8,4,256]{2,1,0:T(4,128)} %param.21, f32[8,4,256]{2,1,0:T(4,128)} %param.20, bf16[8,256,2048]{2,1,0:T(8,128)(2,1)} %param.15, bf16[4,2048]{1,0:T(4,128)(2,1)} %param.18, f32[4]{0:T(128)} %param.19), kind=kOutput, calls=%fused_computation.31 | convolution fusion | flops 33644544 | bytes 8503312 | tf_op jit(solution)/shard_map/spd,hd->shp/dot_general | solution.py:33
  7.0 7.3 %all-to-all-start.1 = ((f32[8,4,256]{2,1,0:T(4,128)}), f32[8,4,256]{2,1,0:T(4,128)S(1)}, u32[]{:S(2)}, u32[]{:S(2)}) async-start(f32[8,4,256]{2,1,0:T(4,128)} %fusion.20), calls=%async_computation.1 | async-start | bytes 65536 | tf_op jit(solution)/shard_map/all_to_all | solution.py:97
  14.3 0.0 copy-done
  14.3 0.0 copy-start.2
  14.4 0.0 copy-start.9
  14.4 5.9 %multiply_reduce_fusion = (f32[8,256,4]{1,2,0:T(4,128)S(1)}, f32[8,256,256]{1,2,0:T(8,128)S(1)}) fusion(bf16[8,256,2048]{2,1,0:T(8,128)(2,1)} %param.15, bf16[2048,256]{1,0:T(8,128)(2,1)S(1)} %copy-done), kind=kOutput, calls=%fused_computation.11 | convolution fusion | flops 2148524032 | bytes 11567104 | tf_op jit(solution)/shard_map/spd,dc->spc/dot_general | solution.py:18
  20.3 0.0 copy-done.2
  20.3 0.0 copy-done.9
  20.4 0.0 copy-start.8
  20.4 2.4 %convolution_convert_fusion = bf16[8,256,256]{1,2,0:T(8,128)(2,1)S(1)} fusion(bf16[8,256,2048]{2,1,0:T(8,128)(2,1)S(1)} %copy-done.2, bf16[2048,256]{1,0:T(8,128)(2,1)S(1)} %copy-done.9), kind=kOutput, calls=%fused_computation.12 | convolution fusion | flops 2148007936 | bytes 10485760 | tf_op jit(solution)/shard_map/spd,dc->spc/dot_general | solution.py:28
  22.8 0.0 copy-done.8
  22.8 0.6 multiply_convert_fusion
  23.4 1.5 %pad_maximum_fusion = bf16[8,256,4,128]{1,3,2,0:T(8,128)(2,1)} fusion(bf16[8,256,4,64]{1,3,2,0:T(8,128)(2,1)S(1)} %bitcast.80, bf16[8,256,4,64]{1,3,2,0:T(8,128)(2,1)S(1)} %multiply_convert_fusion), kind=kLoop, calls=%fused_computation.9 | loop fusion | flops 4194304 | bytes 4194304 | tf_op jit(solution)/shard_map/concatenate | solution.py:32
  24.8 0.0 all-to-all-done.1
  24.9 6.0 %all-to-all-start = ((bf16[8,256,4,128]{1,3,2,0:T(8,128)(2,1)}), bf16[8,256,4,128]{1,3,2,0:T(8,128)(2,1)S(1)}, u32[]{:S(2)}, u32[]{:S(2)}) async-start(bf16[8,256,4,128]{1,3,2,0:T(8,128)(2,1)} %pad_maximum_fusion), calls=%async_computation | async-start | bytes 4194304 | tf_op jit(solution)/shard_map/all_to_all | solution.py:96
  30.8 20.9 %fusion.26 = (bf16[1,14336,4,64]{3,2,1,0:T(4,128)(2,1)}, bf16[1,14336,4,64]{3,2,1,0:T(4,128)(2,1)}) fusion(bf16[1,14336,4,128]{3,2,1,0:T(4,128)(2,1)} %param.22), kind=kLoop, calls=%fused_computation.56 | loop fusion | bytes 29360128 | tf_op jit(solution)/shard_map/slice | solution.py:49
  51.8 0.7 dynamic-slice_reduce_fusion
  52.5 0.1 reshape.260
  52.6 21.4 %copy.37 = bf16[1,14336,4,64]{1,3,2,0:T(8,128)(2,1)} copy(bf16[1,14336,4,64]{3,2,1,0:T(4,128)(2,1)} %get-tuple-element.9) | data formatting | bytes 14680064
  74.1 0.1 reshape.276
  74.1 21.4 %copy.38 = bf16[1,14336,4,64]{1,3,2,0:T(8,128)(2,1)} copy(bf16[1,14336,4,64]{3,2,1,0:T(4,128)(2,1)} %get-tuple-element.10) | data formatting | bytes 14680064
  95.6 0.0 copy-done.7
  95.6 0.1 reshape.269
  95.7 0.0 copy-done.3
  95.7 0.2 slice_reduce_fusion.2
  95.9 0.1 fusion.29
  96.0 1.2 reduce-window.6
  97.2 0.2 slice_reduce_fusion
  97.4 0.2 reduce-window.9
  97.6 0.1 broadcast.92
  97.7 0.1 add_add_fusion
  97.7 0.2 slice_reduce_fusion.1
  97.9 0.1 broadcast_bitcast_fusion
  98.0 0.1 fusion.21
  98.1 4.9 %fusion.27 = (f32[4,2]{1,0:T(4,128)S(1)}, f32[4,2,14336]{2,1,0:T(2,128)}) fusion(f32[4,14336]{1,0:T(4,128)S(1)} %bitcast.79, f32[4]{0:T(128)S(1)} %fusion.25, bf16[4,2,64]{2,1,0:T(2,128)(2,1)S(1)} %reshape.260, bf16[1,14336,4,64]{1,3,2,0:T(8,128)(2,1)} %copy.37), kind=kOutput, calls=%fused_computation.57 | convolution fusion | flops 15138808 | bytes 8029232 | tf_op jit(solution)/shard_map/skge,slke->skgl/dot_general | solution.py:50
  103.0 0.0 all-to-all-done
  103.0 2.5 %copy.26 = bf16[8,256,4,128]{1,0,3,2:T(8,128)(2,1)} copy(bf16[8,256,4,128]{1,3,2,0:T(8,128)(2,1)S(1)} %all-to-all-done) | data formatting | bytes 4194304 | tf_op jit(solution)/shard_map/all_to_all | solution.py:96
  105.5 3.0 %all_to_all.21 = bf16[1,2048,4,128]{1,3,2,0:T(8,128)(2,1)S(1)} reshape(bf16[8,256,4,128]{1,0,3,2:T(8,128)(2,1)} %copy.26) | data formatting | bytes 4194304 | tf_op jit(solution)/shard_map/all_to_all | solution.py:96
  108.5 0.0 copy-done.4
  108.5 0.0 copy-start.5
  108.5 2.5 %copy.30 = bf16[1,2048,4,128]{3,2,1,0:T(4,128)(2,1)} copy(bf16[1,2048,4,128]{1,3,2,0:T(8,128)(2,1)S(1)} %all_to_all.21) | data formatting | bytes 4194304
  111.1 0.3 fusion.28
  111.4 5.3 %fusion.11 = f32[4,2,64]{2,1,0:T(2,128)S(1)} fusion(bf16[1,14336,4,64]{1,3,2,0:T(8,128)(2,1)} %copy.38, f32[4,2,14336]{2,1,0:T(2,128)} %get-tuple-element.17, f32[4,2]{1,0:T(4,128)S(1)} %get-tuple-element.16, f32[4,2]{1,0:T(4,128)S(1)} %get-tuple-element.13), kind=kOutput, calls=%fused_computation.19 | convolution fusion | flops 14909952 | bytes 7800896 | tf_op jit(solution)/shard_map/skgl,slke->skge/dot_general | solution.py:61
  116.7 0.5 multiply_reduce_fusion.1
  117.3 0.1 broadcast_multiply_fusion
  117.3 0.1 reshape.268
  117.4 0.6 convert_element_type.52
  (22 shorter events, 0.2 us)
Async XLA Ops:
  0.6 13.7 %copy-start = (bf16[2048,256]{1,0:T(8,128)(2,1)S(1)}, bf16[2048,256]{1,0:T(8,128)(2,1)}, u32[]{:S(2)}) copy-start(bf16[2048,256]{1,0:T(8,128)(2,1)} %param.16) | copy-start | bytes 3145732
  7.0 17.8 %all-to-all-start.1 = ((f32[8,4,256]{2,1,0:T(4,128)}), f32[8,4,256]{2,1,0:T(4,128)S(1)}, u32[]{:S(2)}, u32[]{:S(2)}) async-start(f32[8,4,256]{2,1,0:T(4,128)} %fusion.20), calls=%async_computation.1 | async-start | bytes 65536 | tf_op jit(solution)/shard_map/all_to_all | solution.py:97
  14.3 6.0 %copy-start.2 = (bf16[8,256,2048]{2,1,0:T(8,128)(2,1)S(1)}, bf16[8,256,2048]{2,1,0:T(8,128)(2,1)}, u32[]{:S(2)}) copy-start(bf16[8,256,2048]{2,1,0:T(8,128)(2,1)} %param.15) | copy-start | bytes 25165828
  14.4 6.0 %copy-start.9 = (bf16[2048,256]{1,0:T(8,128)(2,1)S(1)}, bf16[2048,256]{1,0:T(8,128)(2,1)}, u32[]{:S(2)}) copy-start(bf16[2048,256]{1,0:T(8,128)(2,1)} %param.17) | copy-start | bytes 3145732
  20.4 2.4 %copy-start.8 = (f32[64]{0:T(128)S(1)}, f32[64]{0:T(128)}, u32[]{:S(2)}) copy-start(f32[64]{0:T(128)} %param.28) | copy-start | bytes 772
  24.9 78.2 %all-to-all-start = ((bf16[8,256,4,128]{1,3,2,0:T(8,128)(2,1)}), bf16[8,256,4,128]{1,3,2,0:T(8,128)(2,1)S(1)}, u32[]{:S(2)}, u32[]{:S(2)}) async-start(bf16[8,256,4,128]{1,3,2,0:T(8,128)(2,1)} %pad_maximum_fusion), calls=%async_computation | async-start | bytes 4194304 | tf_op jit(solution)/shard_map/all_to_all | solution.py:96
  52.6 21.4 %copy-start.6 = (bf16[1,256]{1,0:T(2,128)(2,1)S(1)}, bf16[1,256]{1,0:T(2,128)(2,1)}, u32[]{:S(2)}) copy-start(bf16[1,256]{1,0:T(2,128)(2,1)} %param.25) | copy-start | bytes 1540
  74.1 21.5 %copy-start.7 = (bf16[1,256]{1,0:T(2,128)(2,1)S(1)}, bf16[1,256]{1,0:T(2,128)(2,1)}, u32[]{:S(2)}) copy-start(bf16[1,256]{1,0:T(2,128)(2,1)} %param.26) | copy-start | bytes 1540
  74.1 21.6 %copy-start.3 = (f32[1,4,14336]{2,1,0:T(4,128)S(1)}, f32[1,4,14336]{2,1,0:T(4,128)}, u32[]{:S(2)}) copy-start(f32[1,4,14336]{2,1,0:T(4,128)} %param.23) | copy-start | bytes 688132
  74.1 23.8 %copy-start.10 = (f32[1,4]{1,0:T(1,128)S(1)}, f32[1,4]{1,0:T(1,128)}, u32[]{:S(2)}) copy-start(f32[1,4]{1,0:T(1,128)} %param.27) | copy-start | bytes 52
  97.7 10.8 %copy-start.4 = (f32[1,4,2048]{2,1,0:T(4,128)}, f32[1,4,2048]{2,1,0:T(4,128)S(1)}, u32[]{:S(2)}) copy-start(f32[1,4,2048]{2,1,0:T(4,128)S(1)} %add_add_fusion) | copy-start | bytes 98308
  105.5 12.5 %copy-start.1 = (bf16[2048,256]{1,0:T(8,128)(2,1)S(1)}, bf16[2048,256]{1,0:T(8,128)(2,1)}, u32[]{:S(2)}) copy-start(bf16[2048,256]{1,0:T(8,128)(2,1)} %param.16) | copy-start | bytes 3145732
  108.5 8.9 %copy-start.5 = (f32[512]{0:T(512)S(1)}, f32[512]{0:T(512)}, u32[]{:S(2)}) copy-start(f32[512]{0:T(512)} %param.29) | copy-start | bytes 6148
where the time goes:
time: 119 us; the launch traced here: 118 us
  local copies, waits for them, and re-layouts  74.3 us (62%)
  matrix products  25.9 us (22%)
  starting transfers between devices  13.3 us (11%)
  other arithmetic  3.72 us (3%)
    unnamed x26, local copies, waits for them, and re-layouts  45.6 us
    slice x1, local copies, waits for them, and re-layouts, head_scores(): key_heads = cache_rows[..., :head_dim]  20.9 us
    all_to_all x1, starting transfers between devices, local(): lax.all_to_all(local_forget_values, 'sp', split_axis=0, concat_axis=2, ti...  7.31 us
    dot_general x1, matrix products, project(): jnp.einsum('spd,hd->shp', tok_rows, forget_gate_weight, preferred_element...  6.38 us
    all_to_all x1, starting transfers between devices, local(): lax.all_to_all(rows_local, 'sp', split_axis=0, concat_axis=1, tiled=True)  5.99 us
    dot_general x1, matrix products, project(): jnp.einsum('spd,dc->spc', tok_rows, key_projection_weight, preferred_elem...  5.92 us
    dot_general x2, matrix products, weigh(): jnp.einsum('skgl,slke->skge', weights, value_heads, preferred_element_typ...  5.84 us
    all_to_all x2, local copies, waits for them, and re-layouts, local(): lax.all_to_all(rows_local, 'sp', split_axis=0, concat_axis=1, tiled=True)  5.47 us
  transfers between devices with their start and end apart: 2, of which 0 were waited for; matrix products, arithmetic and copies ran while one was open for 70% of the time, Pallas kernels for 0%

commit v1 on v0

--- a/solution.py
+++ b/solution.py
@@ -94,8 +94,11 @@
     )
     local_forget_values = forget_value_rows(gate_preactivation, forget_gate_scale, gate_spike_added)
     new_cache = lax.all_to_all(rows_local, "sp", split_axis=0, concat_axis=1, tiled=True)
-    log_forget_value = lax.all_to_all(
-        local_forget_values, "sp", split_axis=0, concat_axis=2, tiled=True
+    log_forget_value = jnp.concatenate(
+        lax.all_to_all(
+            jnp.stack(jnp.split(local_forget_values, lax.axis_size("sp"), axis=0)), "sp", 0, 0
+        ),
+        axis=2,
     )
     new_logc = prior_cumulative_log_forget[:, :, -1:] + jnp.cumsum(log_forget_value, axis=-1)
     final_logc = new_logc[:, :, -1] + decoded_log_gate

time: 119 us -> 124 us (1.042)
  local copies, waits for them, and re-layouts: 74.3 us -> 79 us
    unnamed x26 -> x33, local copies, waits for them, and re-layouts: 45.6 us -> 49.7 us
  transfers between devices with their start and end apart: 2 -> 2, of which waited for: 0 -> 0; matrix products, arithmetic and copies ran while one was open for 70% -> 68% of each run, Pallas kernels for 0% -> 0%
where the time goes in v1:
time: 124 us; the launch traced here: 122 us
  local copies, waits for them, and re-layouts  79 us (64%)
  matrix products  25.3 us (20%)
  starting transfers between devices  13.3 us (11%)
  other arithmetic  3.72 us (3%)
    unnamed x33, local copies, waits for them, and re-layouts  49.7 us
    slice x1, local copies, waits for them, and re-layouts, head_scores(): key_heads = cache_rows[..., :head_dim]  20.9 us
    all_to_all x1, starting transfers between devices, local(): lax.all_to_all(jnp.stack(jnp.split(local_forget_values, lax.axis_size('sp...  7.31 us
    all_to_all x1, starting transfers between devices, local(): lax.all_to_all(rows_local, 'sp', split_axis=0, concat_axis=1, tiled=True)  5.97 us
    dot_general x1, matrix products, project(): jnp.einsum('spd,dc->spc', tok_rows, key_projection_weight, preferred_elem...  5.93 us
    dot_general x2, matrix products, weigh(): jnp.einsum('skgl,slke->skge', weights, value_heads, preferred_element_typ...  5.84 us
    dot_general x1, matrix products, project(): jnp.einsum('spd,hd->shp', tok_rows, forget_gate_weight, preferred_element...  5.77 us
    all_to_all x2, local copies, waits for them, and re-layouts, local(): lax.all_to_all(rows_local, 'sp', split_axis=0, concat_axis=1, tiled=True)  5.47 us
  transfers between devices with their start and end apart: 2, of which 0 were waited for; matrix products, arithmetic and copies ran while one was open for 68% of the time, Pallas kernels for 0%

profile of v1, /device:TPU:0, one launch (start us, length us, event | category | flops | bytes accessed | tf_op | source)
XLA Modules:
  0.0 122.2 jit_solution(6102530760806221383)
XLA Ops:
  0.6 0.0 copy-start
  0.6 5.8 %fusion.20 = f32[8,4,256]{2,1,0:T(4,128)S(1)} fusion(f32[8,4,256]{2,1,0:T(4,128)} %param.21, f32[8,4,256]{2,1,0:T(4,128)} %param.20, bf16[8,256,2048]{2,1,0:T(8,128)(2,1)} %param.15, bf16[4,2048]{1,0:T(4,128)(2,1)} %param.18, f32[4]{0:T(128)} %param.19), kind=kOutput, calls=%fused_computation.31 | convolution fusion | flops 33644544 | bytes 8503312 | tf_op jit(solution)/shard_map/spd,hd->shp/dot_general | solution.py:33
  6.4 0.6 constant_dynamic-update-slice_fusion.7
  7.0 0.6 constant_dynamic-update-slice_fusion.6
  7.6 0.6 constant_dynamic-update-slice_fusion.5
  8.2 0.6 constant_dynamic-update-slice_fusion.4
  8.8 0.6 constant_dynamic-update-slice_fusion.3
  9.4 0.6 constant_dynamic-update-slice_fusion.2
  10.0 0.6 constant_dynamic-update-slice_fusion.1
  10.6 0.6 constant_dynamic-update-slice_fusion
  11.2 7.3 %all-to-all-start.1 = ((f32[8,1,4,256]{3,2,1,0:T(4,128)}), f32[8,1,4,256]{3,2,1,0:T(4,128)S(1)}, u32[]{:S(2)}, u32[]{:S(2)}) async-start(f32[8,1,4,256]{3,2,1,0:T(4,128)} %constant_dynamic-update-slice_fusion), calls=%async_computation.1 | async-start | bytes 65536 | tf_op jit(solution)/shard_map/all_to_all | solution.py:98
  18.5 0.0 copy-start.2
  18.5 0.0 copy-start.9
  18.5 5.9 %multiply_reduce_fusion = (f32[8,256,4]{1,2,0:T(4,128)S(1)}, f32[8,256,256]{1,2,0:T(8,128)S(1)}) fusion(bf16[8,256,2048]{2,1,0:T(8,128)(2,1)} %param.15, bf16[2048,256]{1,0:T(8,128)(2,1)S(1)} %copy-done), kind=kOutput, calls=%fused_computation.11 | convolution fusion | flops 2148524032 | bytes 11567104 | tf_op jit(solution)/shard_map/spd,dc->spc/dot_general | solution.py:18
  24.5 0.0 copy-start.8
  24.5 2.4 %convolution_convert_fusion = bf16[8,256,256]{1,2,0:T(8,128)(2,1)S(1)} fusion(bf16[8,256,2048]{2,1,0:T(8,128)(2,1)S(1)} %copy-done.2, bf16[2048,256]{1,0:T(8,128)(2,1)S(1)} %copy-done.9), kind=kOutput, calls=%fused_computation.12 | convolution fusion | flops 2148007936 | bytes 10485760 | tf_op jit(solution)/shard_map/spd,dc->spc/dot_general | solution.py:28
  26.9 0.6 multiply_convert_fusion
  27.5 1.5 %pad_maximum_fusion = bf16[8,256,4,128]{1,3,2,0:T(8,128)(2,1)} fusion(bf16[8,256,4,64]{1,3,2,0:T(8,128)(2,1)S(1)} %bitcast.110, bf16[8,256,4,64]{1,3,2,0:T(8,128)(2,1)S(1)} %multiply_convert_fusion), kind=kLoop, calls=%fused_computation.9 | loop fusion | flops 4194304 | bytes 4194304 | tf_op jit(solution)/shard_map/concatenate | solution.py:32
  29.0 0.0 all-to-all-done.1
  29.0 6.0 %all-to-all-start = ((bf16[8,256,4,128]{1,3,2,0:T(8,128)(2,1)}), bf16[8,256,4,128]{1,3,2,0:T(8,128)(2,1)S(1)}, u32[]{:S(2)}, u32[]{:S(2)}) async-start(bf16[8,256,4,128]{1,3,2,0:T(8,128)(2,1)} %pad_maximum_fusion), calls=%async_computation | async-start | bytes 4194304 | tf_op jit(solution)/shard_map/all_to_all | solution.py:96
  35.0 20.9 %fusion.26 = (bf16[1,14336,4,64]{3,2,1,0:T(4,128)(2,1)}, bf16[1,14336,4,64]{3,2,1,0:T(4,128)(2,1)}) fusion(bf16[1,14336,4,128]{3,2,1,0:T(4,128)(2,1)} %param.22), kind=kLoop, calls=%fused_computation.72 | loop fusion | bytes 29360128 | tf_op jit(solution)/shard_map/slice | solution.py:49
  55.9 0.7 dynamic-slice_reduce_fusion
  56.6 0.1 reshape.265
  56.7 21.4 %copy.37 = bf16[1,14336,4,64]{1,3,2,0:T(8,128)(2,1)} copy(bf16[1,14336,4,64]{3,2,1,0:T(4,128)(2,1)} %get-tuple-element.9) | data formatting | bytes 14680064
  78.2 0.1 reshape.281
  78.3 21.4 %copy.38 = bf16[1,14336,4,64]{1,3,2,0:T(8,128)(2,1)} copy(bf16[1,14336,4,64]{3,2,1,0:T(4,128)(2,1)} %get-tuple-element.10) | data formatting | bytes 14680064
  99.8 0.1 reshape.274
  99.8 0.2 slice_reduce_fusion.2
  100.0 0.1 fusion.29
  100.2 1.2 reduce-window.6
  101.3 0.2 slice_reduce_fusion
  101.5 0.2 reduce-window.9
  101.7 0.1 broadcast.92
  101.8 0.1 add_add_fusion
  101.9 0.2 slice_reduce_fusion.1
  102.1 0.1 broadcast_bitcast_fusion
  102.1 0.1 fusion.21
  102.2 4.9 %fusion.27 = (f32[4,2]{1,0:T(4,128)S(1)}, f32[4,2,14336]{2,1,0:T(2,128)}) fusion(f32[4,14336]{1,0:T(4,128)S(1)} %bitcast.109, f32[4]{0:T(128)S(1)} %fusion.25, bf16[4,2,64]{2,1,0:T(2,128)(2,1)S(1)} %reshape.265, bf16[1,14336,4,64]{1,3,2,0:T(8,128)(2,1)} %copy.37), kind=kOutput, calls=%fused_computation.73 | convolution fusion | flops 15138808 | bytes 8029232 | tf_op jit(solution)/shard_map/skge,slke->skgl/dot_general | solution.py:50
  107.2 2.5 %copy.26 = bf16[8,256,4,128]{1,0,3,2:T(8,128)(2,1)} copy(bf16[8,256,4,128]{1,3,2,0:T(8,128)(2,1)S(1)} %all-to-all-done) | data formatting | bytes 4194304 | tf_op jit(solution)/shard_map/all_to_all | solution.py:96
  109.7 3.0 %all_to_all.13 = bf16[1,2048,4,128]{1,3,2,0:T(8,128)(2,1)S(1)} reshape(bf16[8,256,4,128]{1,0,3,2:T(8,128)(2,1)} %copy.26) | data formatting | bytes 4194304 | tf_op jit(solution)/shard_map/all_to_all | solution.py:96
  112.6 0.0 copy-start.5
  112.7 2.5 %copy.30 = bf16[1,2048,4,128]{3,2,1,0:T(4,128)(2,1)} copy(bf16[1,2048,4,128]{1,3,2,0:T(8,128)(2,1)S(1)} %all_to_all.13) | data formatting | bytes 4194304
  115.2 0.3 fusion.28
  115.6 5.3 %fusion.11 = f32[4,2,64]{2,1,0:T(2,128)S(1)} fusion(bf16[1,14336,4,64]{1,3,2,0:T(8,128)(2,1)} %copy.38, f32[4,2,14336]{2,1,0:T(2,128)} %get-tuple-element.17, f32[4,2]{1,0:T(4,128)S(1)} %get-tuple-element.16, f32[4,2]{1,0:T(4,128)S(1)} %get-tuple-element.13), kind=kOutput, calls=%fused_computation.19 | convolution fusion | flops 14909952 | bytes 7800896 | tf_op jit(solution)/shard_map/skgl,slke->skge/dot_general | solution.py:61
  120.9 0.5 multiply_reduce_fusion.1
  121.4 0.1 broadcast_multiply_fusion
  121.5 0.1 reshape.273
  121.6 0.6 convert_element_type.52
  (30 shorter events, 0.2 us)
Async XLA Ops:
  0.6 17.9 %copy-start = (bf16[2048,256]{1,0:T(8,128)(2,1)S(1)}, bf16[2048,256]{1,0:T(8,128)(2,1)}, u32[]{:S(2)}) copy-start(bf16[2048,256]{1,0:T(8,128)(2,1)} %param.16) | copy-start | bytes 3145732
  11.2 17.8 %all-to-all-start.1 = ((f32[8,1,4,256]{3,2,1,0:T(4,128)}), f32[8,1,4,256]{3,2,1,0:T(4,128)S(1)}, u32[]{:S(2)}, u32[]{:S(2)}) async-start(f32[8,1,4,256]{3,2,1,0:T(4,128)} %constant_dynamic-update-slice_fusion), calls=%async_computation.1 | async-start | bytes 65536 | tf_op jit(solution)/shard_map/all_to_all | solution.py:98
  18.5 6.0 %copy-start.2 = (bf16[8,256,2048]{2,1,0:T(8,128)(2,1)S(1)}, bf16[8,256,2048]{2,1,0:T(8,128)(2,1)}, u32[]{:S(2)}) copy-start(bf16[8,256,2048]{2,1,0:T(8,128)(2,1)} %param.15) | copy-start | bytes 25165828
  18.5 6.0 %copy-start.9 = (bf16[2048,256]{1,0:T(8,128)(2,1)S(1)}, bf16[2048,256]{1,0:T(8,128)(2,1)}, u32[]{:S(2)}) copy-start(bf16[2048,256]{1,0:T(8,128)(2,1)} %param.17) | copy-start | bytes 3145732
  24.5 2.4 %copy-start.8 = (f32[64]{0:T(128)S(1)}, f32[64]{0:T(128)}, u32[]{:S(2)}) copy-start(f32[64]{0:T(128)} %param.28) | copy-start | bytes 772
  29.0 78.2 %all-to-all-start = ((bf16[8,256,4,128]{1,3,2,0:T(8,128)(2,1)}), bf16[8,256,4,128]{1,3,2,0:T(8,128)(2,1)S(1)}, u32[]{:S(2)}, u32[]{:S(2)}) async-start(bf16[8,256,4,128]{1,3,2,0:T(8,128)(2,1)} %pad_maximum_fusion), calls=%async_computation | async-start | bytes 4194304 | tf_op jit(solution)/shard_map/all_to_all | solution.py:96
  56.7 21.4 %copy-start.6 = (bf16[1,256]{1,0:T(2,128)(2,1)S(1)}, bf16[1,256]{1,0:T(2,128)(2,1)}, u32[]{:S(2)}) copy-start(bf16[1,256]{1,0:T(2,128)(2,1)} %param.25) | copy-start | bytes 1540
  78.3 21.5 %copy-start.7 = (bf16[1,256]{1,0:T(2,128)(2,1)S(1)}, bf16[1,256]{1,0:T(2,128)(2,1)}, u32[]{:S(2)}) copy-start(bf16[1,256]{1,0:T(2,128)(2,1)} %param.26) | copy-start | bytes 1540
  78.3 21.6 %copy-start.3 = (f32[1,4,14336]{2,1,0:T(4,128)S(1)}, f32[1,4,14336]{2,1,0:T(4,128)}, u32[]{:S(2)}) copy-start(f32[1,4,14336]{2,1,0:T(4,128)} %param.23) | copy-start | bytes 688132
  78.3 23.8 %copy-start.10 = (f32[1,4]{1,0:T(1,128)S(1)}, f32[1,4]{1,0:T(1,128)}, u32[]{:S(2)}) copy-start(f32[1,4]{1,0:T(1,128)} %param.27) | copy-start | bytes 52
  101.9 10.8 %copy-start.4 = (f32[1,4,2048]{2,1,0:T(4,128)}, f32[1,4,2048]{2,1,0:T(4,128)S(1)}, u32[]{:S(2)}) copy-start(f32[1,4,2048]{2,1,0:T(4,128)S(1)} %add_add_fusion) | copy-start | bytes 98308
  109.7 12.5 %copy-start.1 = (bf16[2048,256]{1,0:T(8,128)(2,1)S(1)}, bf16[2048,256]{1,0:T(8,128)(2,1)}, u32[]{:S(2)}) copy-start(bf16[2048,256]{1,0:T(8,128)(2,1)} %param.16) | copy-start | bytes 3145732
  112.6 8.9 %copy-start.5 = (f32[512]{0:T(512)S(1)}, f32[512]{0:T(512)}, u32[]{:S(2)}) copy-start(f32[512]{0:T(512)} %param.29) | copy-start | bytes 6148
